TPU v7x, 32 devices: a whole 2x2x4 slice. The times are simulated.
32 devices in a mesh: sp: 8 (over z, x), tp: 4 (over y, core).
Axes of the slice: x: 2, y: 2, z: 4, core: 2. Of those that a mesh axis runs over, the one named last changes fastest.
Arguments:
- latent: bfloat16 [4096, 2048], P(('sp', 'tp')), may hold values from -6 to 6
- context: bfloat16 [512, 2048], P('sp'), may hold values from -6 to 6
- conditioning: float32 [2048], P('sp'), may hold values from -6 to 6
- context_conditioning: float32 [2048], P('sp'), may hold values from -6 to 6
- shift_weight: bfloat16 [2048, 2048], P('sp', 'tp'), may hold values from -0.25 to 0.25
- scale_weight: bfloat16 [2048, 2048], P('sp', 'tp'), may hold values from -0.25 to 0.25
- gate_weight: bfloat16 [2048, 2048], P('sp', 'tp'), may hold values from -0.25 to 0.25
- norm_gain: float32 [2048], replicated, may hold values from 0.1 to 1.9
- query_weight: bfloat16 [2048, 2048], P(None, 'tp'), may hold values from -0.125 to 0.125
- key_weight: bfloat16 [2048, 1024], P(None, 'tp'), may hold values from -0.125 to 0.125
- value_weight: bfloat16 [2048, 1024], P(None, 'tp'), may hold values from -0.125 to 0.125
- query_gain: float32 [64], replicated, may hold values from 2 to 64, as said below
- key_gain: float32 [64], replicated, may hold values from 0.1 to 1.9
- context_lift: float32 [32], P('tp'), may hold values from 1.5 to 3
- output_weight: bfloat16 [2048, 2048], P('tp'), may hold values from -0.125 to 0.125
Outputs:
- mixed: bfloat16 [4096, 2048], P(('sp', 'tp'))
Inputs may be any that keep to these rules, and one draw needn't show every extreme that they name: `query_gain`: one gain for each channel of a head.
All inputs are finite; a program needn't handle non-finite values.
Results may differ from a plain program's by a relative error of at most 0.018.
The roundings to bfloat16 on the way count: a program that leaves them out, or rounds other values in their place, can miss the bound.
Values may be sent and summed in bfloat16 or wider, within the bound.
A program may use at most 128 MiB of HBM per device.

v0:
```python
import math

import jax
import jax.numpy as jnp
from jax import lax
from jax.sharding import PartitionSpec as P

HEAD = 64
GRID = 64


EPSILON = 1e-06
ROTARY_BASE = 10000.0


def normalize(values, gain):
    return values * lax.rsqrt(jnp.mean(values * values, axis=-1, keepdims=True) + EPSILON) * gain


def rotary_tables(offset, count):
    position = offset + jnp.arange(count, dtype=jnp.int32)
    grid_row = (position // GRID).astype(jnp.float32)
    grid_column = (position % GRID).astype(jnp.float32)
    quarter = HEAD // 4
    frequency = ROTARY_BASE ** (-jnp.arange(quarter, dtype=jnp.float32) / quarter)
    angles = jnp.concatenate(
        [grid_row[:, None] * frequency, grid_column[:, None] * frequency], axis=1
    )
    return (jnp.repeat(jnp.cos(angles), 2, axis=1), jnp.repeat(jnp.sin(angles), 2, axis=1))


def rotate(values, cos_table, sin_table):
    pairs = values.reshape(values.shape[:-1] + (HEAD // 2, 2))
    turned = jnp.stack([-pairs[..., 1], pairs[..., 0]], axis=-1).reshape(values.shape)
    return values * cos_table[:, None, :] + turned * sin_table[:, None, :]


def absorb(state, queries, keys, values, lift):
    top, total, weighted = state
    scores = (
        jnp.einsum("qkgd,skd->kgqs", queries, keys, preferred_element_type=jnp.float32)
        * HEAD ** (-0.5)
        + lift
    )
    new_top = jnp.maximum(top, jnp.max(scores, axis=-1))
    factor = jnp.exp(top - new_top)
    weights = jnp.exp(scores - new_top[..., None])
    total = total * factor + jnp.sum(weights, axis=-1)
    weighted = weighted * factor[..., None] + jnp.einsum(
        "kgqs,skd->kgqd", weights.astype(jnp.bfloat16), values, preferred_element_type=jnp.float32
    )
    return (new_top, total, weighted)


def shards(
    latent,
    context,
    conditioning,
    context_conditioning,
    shift_weight,
    scale_weight,
    gate_weight,
    norm_gain,
    query_weight,
    key_weight,
    value_weight,
    query_gain,
    key_gain,
    context_lift,
    output_weight,
):
    key_heads = key_weight.shape[1] // HEAD
    query_heads = query_weight.shape[1] // HEAD
    group = query_heads // key_heads
    key_width = key_heads * HEAD
    query_width = query_heads * HEAD
    signals = jnp.stack([jax.nn.silu(conditioning), jax.nn.silu(context_conditioning)]).astype(
        jnp.bfloat16
    )
    partial_terms = jnp.stack(
        [
            jnp.dot(signals, shift_weight, preferred_element_type=jnp.float32),
            jnp.dot(signals, scale_weight, preferred_element_type=jnp.float32),
            jnp.dot(signals, gate_weight, preferred_element_type=jnp.float32),
        ],
        axis=1,
    )
    summed = lax.psum(partial_terms, "sp")
    modulation = lax.all_gather(summed, "tp", axis=2, tiled=True)
    hidden = (
        normalize(latent.astype(jnp.float32), norm_gain) * (1.0 + modulation[0, 1])
        + modulation[0, 0]
    ).astype(jnp.bfloat16)
    piece = lax.all_gather(hidden, "tp", axis=0, tiled=True)
    projected = jnp.concatenate(
        [
            jnp.dot(piece, query_weight, preferred_element_type=jnp.float32),
            jnp.dot(piece, key_weight, preferred_element_type=jnp.float32),
            jnp.dot(piece, value_weight, preferred_element_type=jnp.float32),
        ],
        axis=1,
    )
    length = projected.shape[0]
    cos_table, sin_table = rotary_tables(lax.axis_index("sp") * length, length)
    queries = rotate(
        normalize(projected[:, :query_width].reshape(length, query_heads, HEAD), query_gain),
        cos_table,
        sin_table,
    )
    queries = queries.astype(jnp.bfloat16).reshape(length, key_heads, group, HEAD)
    keys = rotate(
        normalize(
            projected[:, query_width : query_width + key_width].reshape(length, key_heads, HEAD),
            key_gain,
        ),
        cos_table,
        sin_table,
    )
    values = projected[:, query_width + key_width :].astype(jnp.bfloat16)
    packed = jnp.concatenate([keys.astype(jnp.bfloat16).reshape(length, key_width), values], axis=1)
    context_hidden = (
        normalize(context.astype(jnp.float32), norm_gain) * (1.0 + modulation[1, 1])
        + modulation[1, 0]
    ).astype(jnp.bfloat16)
    context_count = context.shape[0]
    context_keys = normalize(
        jnp.dot(context_hidden, key_weight, preferred_element_type=jnp.float32).reshape(
            context_count, key_heads, HEAD
        ),
        key_gain,
    )
    context_values = jnp.dot(
        context_hidden, value_weight, preferred_element_type=jnp.float32
    ).astype(jnp.bfloat16)
    context_packed = lax.all_gather(
        jnp.concatenate(
            [context_keys.astype(jnp.bfloat16).reshape(context_count, key_width), context_values],
            axis=1,
        ),
        "sp",
        axis=0,
        tiled=True,
    )
    context_total = context_packed.shape[0]
    start_state = (
        jnp.full((key_heads, group, length), -jnp.inf, jnp.float32),
        jnp.zeros((key_heads, group, length), jnp.float32),
        jnp.zeros((key_heads, group, length, HEAD), jnp.float32),
    )
    lift = context_lift.reshape(key_heads, group, 1, 1)
    state = absorb(
        start_state,
        queries,
        context_packed[:, :key_width].reshape(context_total, key_heads, HEAD),
        context_packed[:, key_width:].reshape(context_total, key_heads, HEAD),
        lift,
    )
    piece = lax.all_gather(packed, "sp", axis=0, tiled=True)
    count = piece.shape[0]
    block = math.gcd(count, 2048)

    def one_block(index, inner):
        part = lax.dynamic_slice_in_dim(piece, index * block, block, 0)
        return absorb(
            inner,
            queries,
            part[:, :key_width].reshape(block, key_heads, HEAD),
            part[:, key_width:].reshape(block, key_heads, HEAD),
            0.0,
        )

    top, total, weighted = lax.fori_loop(0, count // block, one_block, state)
    attended = weighted / total[..., None]
    attended = (
        jnp.transpose(attended, (2, 0, 1, 3)).reshape(length, query_width).astype(jnp.bfloat16)
    )
    by_rows = lax.all_to_all(attended, "tp", split_axis=0, concat_axis=1, tiled=True)
    projection = jnp.dot(
        by_rows,
        lax.all_gather(output_weight, "tp", axis=0, tiled=True),
        preferred_element_type=jnp.float32,
    )
    return (latent.astype(jnp.float32) + modulation[0, 2] * projection).astype(jnp.bfloat16)


def solution(mesh):
    in_specs = (
        P(("sp", "tp"), None),
        P("sp", None),
        P("sp"),
        P("sp"),
        P("sp", "tp"),
        P("sp", "tp"),
        P("sp", "tp"),
        P(),
        P(None, "tp"),
        P(None, "tp"),
        P(None, "tp"),
        P(),
        P(),
        P("tp"),
        P("tp", None),
    )
    out_specs = P(("sp", "tp"), None)
    return jax.shard_map(shards, mesh=mesh, in_specs=in_specs, out_specs=out_specs, check_vma=False)
```

profile of v0, /device:TPU:1, one launch (start us, length us, event | category | flops | bytes accessed | tf_op | source)
XLA Modules:
  0.0 279.8 jit_solution(9180749674133689789)
XLA Ops:
  6.5 0.8 fusion.43
  7.4 0.7 fusion.44
  8.1 1.1 convolution_bitcast_fusion
  9.2 1.1 convolution_bitcast_fusion.1
  10.3 1.1 convolution_bitcast_fusion.2
  11.4 31.0 %psum.7 = f32[2,3,512]{2,0,1:T(2,128)S(1)} all-reduce(f32[2,3,512]{2,0,1:T(2,128)S(1)} %pad_maximum_fusion.5), channel_id=1, replica_groups=mesh['sp'=8,'tp'=4] {'sp'}, use_global_device_ids=true, to_apply=%region_0.1 | all-reduce | flops 3072 | bytes 24576 | tf_op jit(solution)/shard_map/psum | solution.py:88
  42.4 12.9 %all_gather.15 = f32[2,3,2048]{2,0,1:T(2,128)S(1)} all-gather(f32[2,3,512]{2,0,1:T(2,128)S(1)} %psum.7), channel_id=1, replica_groups=mesh['sp'=8,'tp'=4] {'tp'}, dimensions={2}, use_global_device_ids=true | all-gather | bytes 61440 | tf_op jit(solution)/shard_map/all_gather | solution.py:89
  55.3 0.6 fusion.49
  55.9 1.2 fusion.19
  57.2 2.1 fusion.23
  60.0 0.8 mul.369
  60.8 0.7 mul.320
  61.5 17.6 %all-gather.4.cloned.1.call-done = bf16[512,2048]{1,0:T(8,128)(2,1)} async-done(((bf16[128,2048]{1,0:T(8,128)(2,1)}), bf16[512,2048]{1,0:T(8,128)(2,1)}) %all-gather.4.cloned.1.call-update) | async-done | bytes 2097168 | tf_op jit(solution)/shard_map/all_gather | solution.py:94
  79.2 2.6 bitcast_reduce_fusion.3
  83.3 1.2 reshape.188
  84.5 1.2 fusion.30
  85.7 2.6 convolution_convert_fusion
  88.3 0.8 pad_maximum_fusion.2
  89.2 0.7 all-gather.8.cloned.1.call-update
  90.1 1.6 fusion.50
  91.7 1.6 convolution_convert_fusion.1
  93.3 0.7 mul.348
  94.6 28.6 %all_gather.16 = bf16[512,512]{1,0:T(8,128)(2,1)S(1)} all-gather(bf16[64,512]{1,0:T(8,128)(2,1)S(1)} %pad_maximum_fusion.3), channel_id=1, replica_groups=mesh['sp'=8,'tp'=4] {'sp'}, dimensions={0}, use_global_device_ids=true | all-gather | bytes 589824 | tf_op jit(solution)/shard_map/all_gather | solution.py:135
  123.3 1.3 add.225
  124.6 0.8 copy.44
  125.5 3.5 %bitcast_reduce_fusion.2 = (f32[512,8]{0,1:T(8,128)}, f32[512,512]{0,1:T(8,128)S(1)}) fusion(bf16[512,2048]{1,0:T(8,128)(2,1)} %all-gather.4.cloned.1.call-done, bf16[2048,512]{1,0:T(8,128)(2,1)S(1)} %copy-done), kind=kOutput, calls=%fused_computation.35 | convolution fusion | flops 1074262016 | bytes 5259264 | tf_op jit(solution)/shard_map/dot_general | solution.py:97
  129.6 0.7 add_rsqrt_fusion.1
  130.3 0.6 rsqrt.48
  131.0 1.2 multiply_multiply_fusion
  132.1 0.9 slice_negate_fusion
  133.0 1.9 pad_maximum_fusion
  134.9 1.9 reshape.185
  136.9 1.3 add_convert_fusion
  138.2 2.2 bitcast_reduce_fusion.1
  140.4 1.7 fusion.11
  142.2 2.4 fusion.16
  144.5 23.7 %all-gather.6.cloned.1.call-done = bf16[4096,512]{0,1:T(8,128)(2,1)} async-done(((bf16[512,512]{0,1:T(8,128)(2,1)}), bf16[4096,512]{0,1:T(8,128)(2,1)}) %all-gather.6.cloned.1.call-update) | async-done | bytes 4194320 | tf_op jit(solution)/shard_map/all_gather | solution.py:158
  168.3 87.3 %while.17 = (s32[]{:T(128)}, f32[4,2,512]{2,1,0:T(2,128)S(1)}, f32[4,2,512]{2,1,0:T(2,128)S(1)}, f32[4,2,512,64]{2,3,1,0:T(8,128)S(1)}, bf16[4096,512]{0,1:T(8,1...) while((s32[]{:T(128)}, f32[4,2,512]{2,1,0:T(2,128)S(1)}, ...), condition=%wide.region_11.12_spmd, body=%wide.region_8.11_spmd.sunk | while | flops 2215124992 | bytes 109838512 | solution.py:172
  168.3 1.8 fusion.81
  170.1 15.8 %bitcast_reduce_fusion.5 = (f32[4,2,512]{2,1,0:T(2,128)S(1)}, f32[4,2048,512,2]{2,1,3,0:T(8,128)}) fusion(bf16[2048,4,64,1]{0,2,3,1:T(8,128)(2,1)S(1)} %bitcast.152, bf16[512,4,2,64]{0,3,2,1:T(8,128)(2,1)S(1)} %get-tuple-element.242), kind=kOutput, calls=%fused_computation.1.clone.1 | convolution fusion | flops 1090514944 | bytes 35143680 | tf_op jit(solution)/shard_map/while/body/eval_jaxpr/qkgd,skd->kgqs/dot_general | solution.py:41
  185.9 13.7 %fusion.82 = f32[4,2,512]{2,1,0:T(2,128)S(1)} fusion(f32[4,2048,512,2]{2,1,3,0:T(8,128)} %get-tuple-element.211, f32[4,2,512]{2,1,0:T(2,128)S(1)} %max.8), kind=kLoop, calls=%fused_computation.4.clone.1 | loop fusion | flops 25161728 | bytes 33587200 | tf_op jit(solution)/shard_map/while/body/eval_jaxpr/reduce_sum | solution.py:48
  199.6 13.7 %fusion.83 = f32[4,2,512,64]{2,3,1,0:T(8,128)S(1)} fusion(bf16[2048,4,64,1]{0,2,3,1:T(8,128)(2,1)S(1)} %bitcast.153, f32[4,2048,512,2]{2,1,3,0:T(8,128)} %get-tuple-element.211, f32[4,2,512]{2,1,0:T(2,128)S(1)} %max.8, f32[4,2,512,64]{2,3,1,0:T(8,128)S(1)} %get-tuple-element.229, f32[4,2,512]{2,1,0:T(2,128)S(1)} %bitcast.159), kind=kOutput, calls=%fused_computation.6.clone.1 | convolution fusion | flops 1099431936 | bytes 36732928 | tf_op jit(solution)/shard_map/while/body/eval_jaxpr/kgqs,skd->kgqd/dot_general | solution.py:49
  213.4 1.7 fusion.81
  215.1 13.3 %bitcast_reduce_fusion.5 = (f32[4,2,512]{2,1,0:T(2,128)S(1)}, f32[4,2048,512,2]{2,1,3,0:T(8,128)}) fusion(bf16[2048,4,64,1]{0,2,3,1:T(8,128)(2,1)S(1)} %bitcast.152, bf16[512,4,2,64]{0,3,2,1:T(8,128)(2,1)S(1)} %get-tuple-element.242), kind=kOutput, calls=%fused_computation.1.clone.1 | convolution fusion | flops 1090514944 | bytes 35143680 | tf_op jit(solution)/shard_map/while/body/eval_jaxpr/qkgd,skd->kgqs/dot_general | solution.py:41
  228.4 13.6 %fusion.82 = f32[4,2,512]{2,1,0:T(2,128)S(1)} fusion(f32[4,2048,512,2]{2,1,3,0:T(8,128)} %get-tuple-element.211, f32[4,2,512]{2,1,0:T(2,128)S(1)} %max.8), kind=kLoop, calls=%fused_computation.4.clone.1 | loop fusion | flops 25161728 | bytes 33587200 | tf_op jit(solution)/shard_map/while/body/eval_jaxpr/reduce_sum | solution.py:48
  242.0 13.5 %fusion.83 = f32[4,2,512,64]{2,3,1,0:T(8,128)S(1)} fusion(bf16[2048,4,64,1]{0,2,3,1:T(8,128)(2,1)S(1)} %bitcast.153, f32[4,2048,512,2]{2,1,3,0:T(8,128)} %get-tuple-element.211, f32[4,2,512]{2,1,0:T(2,128)S(1)} %max.8, f32[4,2,512,64]{2,3,1,0:T(8,128)S(1)} %get-tuple-element.229, f32[4,2,512]{2,1,0:T(2,128)S(1)} %bitcast.159), kind=kOutput, calls=%fused_computation.6.clone.1 | convolution fusion | flops 1099431936 | bytes 36732928 | tf_op jit(solution)/shard_map/while/body/eval_jaxpr/kgqs,skd->kgqd/dot_general | solution.py:49
  255.9 11.9 %all_to_all.16 = bf16[4,128,512]{1,2,0:T(8,128)(2,1)S(1)} all-to-all(bf16[4,128,512]{1,2,0:T(8,128)(2,1)S(1)} %copy.46), channel_id=1, replica_groups=mesh['sp'=8,'tp'=4] {'tp'}, dimensions={0} | all-to-all | bytes 1048576 | tf_op jit(solution)/shard_map/all_to_all | solution.py:177
  267.8 5.5 %fusion.15 = bf16[128,2048]{1,0:T(8,128)(2,1)} fusion(bf16[128,2048]{0,1:T(8,128)(2,1)S(1)} %bitcast.156, bf16[2048,2048]{1,0:T(8,128)(2,1)} %all-gather.8.cloned.1.call-done, bf16[128,2048]{1,0:T(8,128)(2,1)S(1)} %copy-done.2, f32[2048]{0:T(1024)S(1)} %bitcast.164), kind=kOutput, calls=%fused_computation.20 | convolution fusion | flops 1074790400 | bytes 9969664 | tf_op jit(solution)/shard_map/dot_general | solution.py:178
  (66 shorter events, 4.3 us)
Async XLA Ops:
  6.5 119.0 %copy-start = (bf16[2048,512]{1,0:T(8,128)(2,1)S(1)}, bf16[2048,512]{1,0:T(8,128)(2,1)}, u32[]{:S(2)}) copy-start(bf16[2048,512]{1,0:T(8,128)(2,1)} %param.25) | copy-start | bytes 6291460
  6.5 72.6 %all-gather.4.cloned.1.call-start = ((), (), s32[]{:S(2)}) async-start(), calls=%async_computation.1 | async-start | bytes 2621440 | tf_op jit(solution)/shard_map/all_gather | solution.py:94
  59.3 109.0 %all-gather.6.cloned.1.call-start = ((), (), s32[]{:S(2)}) async-start(), calls=%async_computation.2 | async-start | bytes 4718592 | tf_op jit(solution)/shard_map/all_gather | solution.py:158
  60.0 29.9 %copy-start.3 = (f32[512,64]{0,1:T(8,128)}, f32[512,64]{0,1:T(8,128)S(1)}, u32[]{:S(2)}) copy-start(f32[512,64]{0,1:T(8,128)S(1)} %mul.351) | copy-start | bytes 393220
  61.5 28.6 %copy-start.7 = (f32[2048]{0:T(1024)S(1)}, f32[2048]{0:T(1024)}, u32[]{:S(2)}) copy-start(f32[2048]{0:T(1024)} %param.24) | copy-start | bytes 24580
  82.1 11.1 %copy-start.9 = (f32[64]{0:T(128)S(1)}, f32[64]{0:T(128)}, u32[]{:S(2)}) copy-start(f32[64]{0:T(128)} %param.28) | copy-start | bytes 772
  84.5 5.5 %copy-start.4 = (bf16[64,2048]{1,0:T(8,128)(2,1)S(1)}, bf16[64,2048]{1,0:T(8,128)(2,1)}, u32[]{:S(2)}) copy-start(bf16[64,2048]{1,0:T(8,128)(2,1)} %param.18) | copy-start | bytes 786436
  89.2 178.6 %all-gather.8.cloned.1.call-start = ((), (), s32[]{:S(2)}) async-start(), calls=%async_computation.3 | async-start | bytes 10485760 | tf_op jit(solution)/shard_map/all_gather | solution.py:180
  136.9 3.5 %copy-start.6 = (f32[4,2]{1,0:T(4,128)S(1)}, f32[4,2]{1,0:T(4,128)}, u32[]{:S(2)}) copy-start(f32[4,2]{1,0:T(4,128)} %add.225) | copy-start | bytes 100
  138.2 4.0 %copy-start.5 = (bf16[512,256]{0,1:T(8,128)(2,1)S(1)}, bf16[512,256]{0,1:T(8,128)(2,1)}, u32[]{:S(2)}) copy-start(bf16[512,256]{0,1:T(8,128)(2,1)} %copy.44) | copy-start | bytes 786436
  168.3 99.5 %copy-start.2 = (bf16[128,2048]{1,0:T(8,128)(2,1)S(1)}, bf16[128,2048]{1,0:T(8,128)(2,1)}, u32[]{:S(2)}) copy-start(bf16[128,2048]{1,0:T(8,128)(2,1)} %param.17) | copy-start | bytes 1572868
  168.3 99.5 %copy-start.8 = (f32[1,1,2048]{2,0,1:T(1,128)S(1)}, f32[1,1,2048]{2,0,1:T(1,128)}, u32[]{:S(2)}) copy-start(f32[1,1,2048]{2,0,1:T(1,128)} %get-tuple-element.143) | copy-start | bytes 24580
  255.9 17.4 %copy-start.1 = (bf16[2048,512]{1,0:T(8,128)(2,1)S(1)}, bf16[2048,512]{1,0:T(8,128)(2,1)}, u32[]{:S(2)}) copy-start(bf16[2048,512]{1,0:T(8,128)(2,1)} %param.25) | copy-start | bytes 6291460
Sparse Core Ops, SparseCore 0:
  59.4 19.7 all-gather.3
  89.3 78.9 all-gather.5
  169.8 57.6 all-gather.7
where the time goes:
time: 282 us; the launch traced here: 280 us
  blocking collectives  84.3 us (30%)
  matrix products  81.5 us (29%)
  other arithmetic  44.6 us (16%)
  waiting for transfers between devices  42.1 us (15%)
  local copies, waits for them, and re-layouts  13.6 us (5%)
  between operations  13.5 us (5%)
    dot_general x3, matrix products, absorb(): jnp.einsum('qkgd,skd->kgqs', queries, keys, preferred_element_type=jnp.fl...  31.3 us
    psum x1, blocking collectives, shards(): summed = lax.psum(partial_terms, 'sp')  31 us
    dot_general x3, matrix products, absorb(): jnp.einsum('kgqs,skd->kgqd', weights.astype(jnp.bfloat16), values, prefer...  29.6 us
    reduce_sum x3, other arithmetic, absorb(): total = total * factor + jnp.sum(weights, axis=-1)  29 us
    all_gather x1, blocking collectives, shards(): lax.all_gather(jnp.concatenate([context_keys.astype(jnp.bfloat16).reshape...  28.6 us
    all_gather x1, waiting for transfers between devices, shards(): piece = lax.all_gather(packed, 'sp', axis=0, tiled=True)  23.7 us
    all_gather x1, waiting for transfers between devices, shards(): piece = lax.all_gather(hidden, 'tp', axis=0, tiled=True)  17.6 us
    all_gather x1, blocking collectives, shards(): modulation = lax.all_gather(summed, 'tp', axis=2, tiled=True)  12.9 us
  transfers between devices with their start and end apart: 3, of which 2 were waited for; matrix products, arithmetic and copies ran while one was open for 41% of the time, Pallas kernels for 0%

commit v1 on v0

v1 whole, which is shorter than its diff:
```python
import functools

import jax
import jax.numpy as jnp
from jax import lax
from jax.experimental import pallas as pl
from jax.experimental.pallas import tpu as pltpu
from jax.sharding import PartitionSpec as P

HEAD = 64
GRID = 64
EPSILON = 1e-06
ROTARY_BASE = 10000.0
F32 = jnp.float32
BF16 = jnp.bfloat16
VMEM = pltpu.VMEM


def dot(a, b):
    return jnp.dot(a, b, preferred_element_type=F32)


def remote(src, dst, send, recv, sp, tp):
    return pltpu.make_async_remote_copy(
        src_ref=src,
        dst_ref=dst,
        send_sem=send,
        recv_sem=recv,
        device_id=(sp, tp),
        device_id_type=pl.DeviceIdType.MESH,
    )


def project_kernel(
    n_sp, n_tp, q_heads, k_heads,
    latent, context, cond, ctx_cond, shift_w, scale_w, gate_w, gain,
    wq, wk, wv, q_gain, k_gain, cos_t, sin_t,
    qz, kv, ckv, gate_out,
    lat, part, total, recv1, recv2, mods,
    s1, r1, s2, r2, sy, ry, sp_own, sp_fwd, rp,
):
    me = lax.axis_index("sp")
    t = lax.axis_index("tp")
    n_y = n_tp // 2
    y, c = t // 2, t % 2
    partner = y * 2 + 1 - c
    barrier = pltpu.get_barrier_semaphore()

    def greet_sp(j, _):
        pl.semaphore_signal(barrier, inc=1, device_id=(lax.rem(me + j, n_sp), t), device_id_type=pl.DeviceIdType.MESH)
        return 0

    def greet_tp(j, _):
        pl.semaphore_signal(barrier, inc=1, device_id=(me, lax.rem(t + j, n_tp)), device_id_type=pl.DeviceIdType.MESH)
        return 0

    lax.fori_loop(1, n_sp, greet_sp, 0)
    lax.fori_loop(1, n_tp, greet_tp, 0)
    pl.semaphore_wait(barrier, n_sp + n_tp - 2)

    def y_copy(k):
        other = lax.rem(y + k, n_y)
        return remote(latent, lat.at[t], sy.at[k], ry.at[t], me, other * 2 + c)

    def y_start(k, _):
        y_copy(k).start()
        return 0

    lax.fori_loop(1, n_y, y_start, 0)
    own_partner = remote(latent, lat.at[t], sp_own, rp.at[t], me, partner)
    own_partner.start()

    rows = lax.broadcasted_iota(jnp.int32, (8, cond.shape[1]), 0)
    a = jnp.broadcast_to(cond[...] / (1.0 + jnp.exp(-cond[...])), rows.shape)
    b = jnp.broadcast_to(ctx_cond[...] / (1.0 + jnp.exp(-ctx_cond[...])), rows.shape)
    first = jnp.where(rows == 0, a, jnp.where(rows == 1, b, 0.0)).astype(BF16)
    second = jnp.where(rows == 2, a, jnp.where(rows == 3, b, 0.0)).astype(BF16)
    third = jnp.where(rows == 4, a, 0.0).astype(BF16)
    mine = dot(first, shift_w[...]) + dot(second, scale_w[...]) + dot(third, gate_w[...])
    part[...] = mine
    recv1[me] = mine

    def mod_copy(j):
        return remote(part, recv1.at[me], s1.at[j], r1.at[me], lax.rem(me + j, n_sp), t)

    def mod_start(j, _):
        mod_copy(j).start()
        return 0

    def mod_wait(j, _):
        src = lax.rem(me + j, n_sp)
        pltpu.make_async_copy(recv1.at[src], recv1.at[src], r1.at[src]).wait()
        return 0

    lax.fori_loop(1, n_sp, mod_start, 0)
    lax.fori_loop(1, n_sp, mod_wait, 0)
    summed = lax.fori_loop(1, n_sp, lambda j, s: s + recv1[j], recv1[0])
    total[...] = summed
    recv2[t] = summed

    def tot_copy(j):
        return remote(total, recv2.at[t], s2.at[j], r2.at[t], me, lax.rem(t + j, n_tp))

    def tot_start(j, _):
        tot_copy(j).start()
        return 0

    def tot_wait(j, _):
        src = lax.rem(t + j, n_tp)
        pltpu.make_async_copy(recv2.at[src], recv2.at[src], r2.at[src]).wait()
        return 0

    lax.fori_loop(1, n_tp, tot_start, 0)
    lax.fori_loop(1, n_tp, tot_wait, 0)
    width = total.shape[1]
    for j in range(n_tp):
        mods[:, j * width : (j + 1) * width] = recv2[j]
    gate_out[...] = mods[4:5, :]

    def hidden_of(x, shift_row, scale_row):
        x = x.astype(F32)
        inv = lax.rsqrt(jnp.mean(x * x, axis=-1, keepdims=True) + EPSILON)
        return (
            x * inv * gain[...] * (1.0 + mods[scale_row : scale_row + 1, :])
            + mods[shift_row : shift_row + 1, :]
        ).astype(BF16)

    def head_norm(v, gains):
        w = v.shape[1]
        heads_r = lax.broadcasted_iota(jnp.int32, (w, w), 0) // HEAD
        heads_c = lax.broadcasted_iota(jnp.int32, (w, w), 1) // HEAD
        ones = jnp.where(heads_r == heads_c, 1.0, 0.0).astype(BF16)
        sq = v * v
        hi = sq.astype(BF16)
        rest = sq - hi.astype(F32)
        mid = rest.astype(BF16)
        low = (rest - mid.astype(F32)).astype(BF16)
        mean = (dot(hi, ones) + (dot(mid, ones) + dot(low, ones))) * (1.0 / HEAD)
        return v * lax.rsqrt(mean + EPSILON) * jnp.concatenate([gains] * (w // 128), axis=1)

    def turn(v, cos_v, sin_v):
        w = v.shape[1]
        even = lax.broadcasted_iota(jnp.int32, v.shape, 1) % 2 == 0
        swapped = jnp.where(even, pltpu.roll(v, w - 1, 1), pltpu.roll(v, 1, 1))
        many = w // 128
        return v * jnp.concatenate([cos_v] * many, axis=1) + swapped * jnp.concatenate([sin_v] * many, axis=1)

    k_width = wk.shape[1]
    group = q_heads // k_heads

    def process(tile, x):
        h = hidden_of(x, 0, 2)
        cos_v, sin_v = cos_t[tile], sin_t[tile]
        q = turn(head_norm(dot(h, wq[...]), q_gain[...]), cos_v, sin_v)
        low_half = lax.broadcasted_iota(jnp.int32, (q.shape[0], 128), 1) < HEAD
        for head in range(q_heads):
            piece = q[:, (head // 2) * 128 : (head // 2) * 128 + 128].astype(BF16).astype(F32) * HEAD ** (-0.5)
            side = (head // group) % 2
            if head % 2 != side:
                piece = pltpu.roll(piece, HEAD, 1)
            keep = low_half if side == 0 else jnp.logical_not(low_half)
            qz[head, tile] = jnp.where(keep, piece, 0.0).astype(BF16)
        k = turn(head_norm(dot(h, wk[...]), k_gain[...]), cos_v, sin_v)
        kv[tile, :, :k_width] = k.astype(BF16)
        kv[tile, :, k_width:] = dot(h, wv[...]).astype(BF16)

    hc = hidden_of(context[...], 1, 3)
    ckv[:, :k_width] = head_norm(dot(hc, wk[...]), k_gain[...]).astype(BF16)
    ckv[:, k_width:] = dot(hc, wv[...]).astype(BF16)

    process(t, latent[...])
    pltpu.make_async_copy(lat.at[partner], lat.at[partner], rp.at[partner]).wait()
    process(partner, lat[partner])

    def others(k, _):
        other = lax.rem(y + n_y - k, n_y)
        near, far = other * 2 + c, other * 2 + 1 - c
        pltpu.make_async_copy(lat.at[near], lat.at[near], ry.at[near]).wait()
        remote(lat.at[near], lat.at[near], sp_fwd.at[k], rp.at[near], me, partner).start()
        process(near, lat[near])
        pltpu.make_async_copy(lat.at[far], lat.at[far], rp.at[far]).wait()
        process(far, lat[far])
        return 0

    lax.fori_loop(1, n_y, others, 0)

    def drain_y(k, _):
        y_copy(k).wait_send()
        other = lax.rem(y + n_y - k, n_y)
        near = other * 2 + c
        remote(lat.at[near], lat.at[near], sp_fwd.at[k], rp.at[near], me, partner).wait_send()
        return 0

    lax.fori_loop(1, n_y, drain_y, 0)
    own_partner.wait_send()

    def drain_1(j, _):
        mod_copy(j).wait_send()
        return 0

    def drain_2(j, _):
        tot_copy(j).wait_send()
        return 0

    lax.fori_loop(1, n_sp, drain_1, 0)
    lax.fori_loop(1, n_tp, drain_2, 0)


def ring_position(index, n_z, n_x):
    z, x = index // n_x, index % n_x
    back = n_z * (n_x - 1) + n_z - 1 - z
    out = z * (n_x - 1) + jnp.where(z % 2 == 0, x - 1, n_x - 1 - x)
    return jnp.where(x == 0, back, out)


def ring_index(place, n_z, n_x):
    r, k = place // (n_x - 1), place % (n_x - 1)
    out = r * n_x + jnp.where(r % 2 == 0, 1 + k, n_x - 1 - k)
    back = (n_z - 1 - (place - n_z * (n_x - 1))) * n_x
    return jnp.where(place >= n_z * (n_x - 1), back, out)


def attend_kernel(
    n_sp, n_tp, n_x, q_heads, k_heads, chunks,
    qz, kv, ckv, lift, wo,
    by_rows, wo_all,
    right, left, cbuf, m_ref, acc, att,
    s_kv, r_kv, s_c, r_c, s_wy, r_wy, s_wp, r_wp, s_a, r_a, loc,
):
    me = lax.axis_index("sp")
    t = lax.axis_index("tp")
    n_y = n_tp // 2
    y, c = t // 2, t % 2
    partner = y * 2 + 1 - c
    half = n_sp // 2
    if n_x > 1:
        n_z = n_sp // n_x
        place = ring_position(me, n_z, n_x)
        nxt = ring_index(lax.rem(place + 1, n_sp), n_z, n_x)
        prv = ring_index(lax.rem(place + n_sp - 1, n_sp), n_z, n_x)
    else:
        nxt, prv = lax.rem(me + 1, n_sp), lax.rem(me + n_sp - 1, n_sp)
    barrier = pltpu.get_barrier_semaphore()
    for peer in (nxt, prv):
        pl.semaphore_signal(barrier, inc=1, device_id=(peer, t), device_id_type=pl.DeviceIdType.MESH)

    def greet(j, _):
        pl.semaphore_signal(barrier, inc=1, device_id=(me, lax.rem(t + j, n_tp)), device_id_type=pl.DeviceIdType.MESH)
        return 0

    lax.fori_loop(1, n_tp, greet, 0)
    pl.semaphore_wait(barrier, 2 + n_tp - 1)

    length = kv.shape[0]
    mid = length // 2

    def hop(src, dst, direction, i):
        return remote(src, dst, s_kv.at[direction, i], r_kv.at[direction, i], nxt if direction == 0 else prv, t)

    def chop(src, dst, direction, i):
        return remote(src, dst, s_c.at[direction, i], r_c.at[direction, i], nxt if direction == 0 else prv, t)

    def sends(i, source_r, source_l, c_r, c_l):
        return (
            hop(source_r, right.at[i], 0, i),
            hop(source_l, left.at[i], 1, i),
            chop(c_r, cbuf.at[i], 0, i),
            chop(c_l, cbuf.at[n_sp - i], 1, i),
        )

    def last_sends(source_r, source_l, c_r):
        return (
            hop(source_r.at[pl.ds(0, mid)], right.at[half, pl.ds(0, mid)], 0, half),
            hop(source_l.at[pl.ds(mid, mid)], right.at[half, pl.ds(mid, mid)], 1, half),
            chop(c_r, cbuf.at[half], 0, half),
        )

    opening = sends(1, kv, kv, ckv, ckv)
    for copy in opening:
        copy.start()
    own_c = pltpu.make_async_copy(ckv, cbuf.at[0], loc.at[0])
    own_c.start()
    own_w = pltpu.make_async_copy(wo, wo_all.at[t], loc.at[1])
    own_w.start()

    def w_y(k, ch):
        other = lax.rem(y + k, n_y)
        return remote(wo.at[ch], wo_all.at[t, ch], s_wy.at[k, ch], r_wy.at[t, ch], me, other * 2 + c)

    def w_own(ch):
        return remote(wo.at[ch], wo_all.at[t, ch], s_wp.at[0, ch], r_wp.at[t, ch], me, partner)

    def w_fwd(k, ch):
        other = lax.rem(y + n_y - k, n_y)
        near = other * 2 + c
        return remote(wo_all.at[near, ch], wo_all.at[near, ch], s_wp.at[k, ch], r_wp.at[near, ch], me, partner)

    for ch in range(chunks):
        for k in range(1, n_y):
            w_y(k, ch).start()
    for ch in range(chunks):
        w_own(ch).start()

    def forward_weight(ch):
        for k in range(1, n_y):
            other = lax.rem(y + n_y - k, n_y)
            near = other * 2 + c
            pltpu.make_async_copy(wo_all.at[near, ch], wo_all.at[near, ch], r_wy.at[near, ch]).wait()
            w_fwd(k, ch).start()

    k_width = kv.shape[1] // 2
    group = q_heads // k_heads
    tile = min(256, length)
    tiles = length // tile

    def attend(blocks, start, lifted):
        def one(step, _):
            head = step // tiles
            row = pl.multiple_of(lax.rem(step, tiles) * tile, tile)
            pair = head // (2 * group)
            lane = pl.multiple_of(pair * 128, 128)
            q = qz[head, pl.ds(row, tile), :]
            extra = lift[head]
            scores = []
            for pos, block in enumerate(blocks):
                s = lax.dot_general(
                    q, block[:, pl.ds(lane, 128)], (((1,), (1,)), ((), ())), preferred_element_type=F32
                )
                scores.append(s)
            tops = [jnp.max(s, axis=-1, keepdims=True) for s in scores]
            if lifted:
                tops[-1] = tops[-1] + extra
            top = functools.reduce(jnp.maximum, tops)
            if not start:
                old = m_ref[head, pl.ds(row, tile), :]
                top = jnp.maximum(old[:, 0:1], top)
            out = None
            for pos, block in enumerate(blocks):
                base = top - extra if lifted and pos == len(blocks) - 1 else top
                p = jnp.exp(scores[pos] - base).astype(BF16)
                v = block[:, pl.ds(pl.multiple_of(k_width + lane, 128), 128)]
                term = dot(p, jnp.concatenate([v, jnp.ones_like(v)], axis=1))
                out = term if out is None else out + term
            if not start:
                wide = jnp.broadcast_to(top, old.shape)
                f = jnp.exp(old - wide)
                out = acc[head, pl.ds(row, tile), :] * jnp.concatenate([f, f], axis=1) + out
                m_ref[head, pl.ds(row, tile), :] = wide
            else:
                m_ref[head, pl.ds(row, tile), :] = jnp.broadcast_to(top, (tile, 128))
            acc[head, pl.ds(row, tile), :] = out
            return 0

        lax.fori_loop(0, q_heads * tiles, one, 0)

    attend([kv], True, False)

    def wait_pair(i):
        for copy in sends(i, kv, kv, ckv, ckv):
            copy.wait_recv()

    def step(i, _):
        wait_pair(i)
        for copy in sends(i + 1, right.at[i], left.at[i], cbuf.at[i], cbuf.at[n_sp - i]):
            copy.start()
        attend([right.at[i], left.at[i]], False, False)
        forward_weight(i - 1)
        return 0

    lax.fori_loop(1, half - 1, step, 0)
    wait_pair(half - 1)
    closing = last_sends(right.at[half - 1], left.at[half - 1], cbuf.at[half - 1])
    for copy in closing:
        copy.start()
    attend([right.at[half - 1], left.at[half - 1]], False, False)
    for ch in range(half - 2, chunks):
        forward_weight(ch)
    for copy in closing:
        copy.wait_recv()
    own_c.wait()
    cflat = cbuf.reshape(n_sp * ckv.shape[0], ckv.shape[1])
    attend([right.at[half], cflat], False, True)

    low_half = lax.broadcasted_iota(jnp.int32, (length, 128), 1) < HEAD
    per = length // n_tp

    def normal(head):
        return acc[head, :, :128] / acc[head, :, 128:]

    for two in range(q_heads // 2):
        parts = []
        for head in (2 * two, 2 * two + 1):
            o = normal(head)
            if (head // group) % 2 != head % 2:
                o = pltpu.roll(o, HEAD, 1)
            parts.append(o)
        both = jnp.where(low_half, parts[0], parts[1]).astype(BF16)
        for j in range(n_tp):
            att[j, :, two * 128 : two * 128 + 128] = both[j * per : (j + 1) * per, :]

    def a_copy(j):
        to = lax.rem(t + j, n_tp)
        return remote(att.at[to], by_rows.at[t], s_a.at[j], r_a.at[t], me, to)

    for j in range(1, n_tp):
        a_copy(j).start()
    own_a = pltpu.make_async_copy(att.at[t], by_rows.at[t], loc.at[2])
    own_a.start()
    own_a.wait()
    for j in range(1, n_tp):
        src = lax.rem(t + j, n_tp)
        pltpu.make_async_copy(by_rows.at[src], by_rows.at[src], r_a.at[src]).wait()
    own_w.wait()
    for ch in range(chunks):
        for k in range(n_y):
            far = lax.rem(y + n_y - k, n_y) * 2 + 1 - c
            pltpu.make_async_copy(wo_all.at[far, ch], wo_all.at[far, ch], r_wp.at[far, ch]).wait()
        for k in range(1, n_y):
            w_y(k, ch).wait_send()
            w_fwd(k, ch).wait_send()
        w_own(ch).wait_send()
    for j in range(1, n_tp):
        a_copy(j).wait_send()

    def drain(i, _):
        for copy in sends(i, kv, kv, ckv, ckv):
            copy.wait_send()
        return 0

    lax.fori_loop(1, half, drain, 0)
    for copy in closing:
        copy.wait_send()


def rotary_tables(offset, count):
    position = offset + jnp.arange(count, dtype=jnp.int32)
    grid_row = (position // GRID).astype(F32)
    grid_column = (position % GRID).astype(F32)
    quarter = HEAD // 4
    frequency = ROTARY_BASE ** (-jnp.arange(quarter, dtype=F32) / quarter)
    angles = jnp.concatenate([grid_row[:, None] * frequency, grid_column[:, None] * frequency], axis=1)
    sign = jnp.where(jnp.arange(HEAD) % 2 == 0, -1.0, 1.0)
    cos_t, sin_t = jnp.repeat(jnp.cos(angles), 2, axis=1), jnp.repeat(jnp.sin(angles), 2, axis=1) * sign
    return jnp.tile(cos_t, (1, 2)), jnp.tile(sin_t, (1, 2))


def shards(
    n_sp, n_tp, n_x,
    latent, context, conditioning, context_conditioning, shift_weight, scale_weight, gate_weight,
    norm_gain, query_weight, key_weight, value_weight, query_gain, key_gain, context_lift, output_weight,
):
    k_heads = key_weight.shape[1] // HEAD
    q_heads = query_weight.shape[1] // HEAD
    if k_heads % 2:
        key_weight = jnp.pad(key_weight, ((0, 0), (0, HEAD)))
        value_weight = jnp.pad(value_weight, ((0, 0), (0, HEAD)))
    rows, model = latent.shape
    length = rows * n_tp
    k_width = key_weight.shape[1]
    c_rows = context.shape[0]
    part_width = shift_weight.shape[1]
    cos_t, sin_t = rotary_tables(lax.axis_index("sp") * length, length)
    vmem = pl.BlockSpec(memory_space=VMEM)
    dma = pltpu.SemaphoreType.DMA
    qz, kv, ckv, gate = pl.pallas_call(
        functools.partial(project_kernel, n_sp, n_tp, q_heads, k_heads),
        name="project",
        out_shape=(
            jax.ShapeDtypeStruct((q_heads, n_tp, rows, 128), BF16),
            jax.ShapeDtypeStruct((n_tp, rows, 2 * k_width), BF16),
            jax.ShapeDtypeStruct((c_rows, 2 * k_width), BF16),
            jax.ShapeDtypeStruct((1, model), F32),
        ),
        in_specs=[vmem] * 15,
        out_specs=(vmem,) * 4,
        scratch_shapes=[
            VMEM((n_tp, rows, model), BF16),
            VMEM((8, part_width), F32),
            VMEM((8, part_width), F32),
            VMEM((n_sp, 8, part_width), F32),
            VMEM((n_tp, 8, part_width), F32),
            VMEM((8, model), F32),
            dma((n_sp,)), dma((n_sp,)), dma((n_tp,)), dma((n_tp,)),
            dma((n_tp,)), dma((n_tp,)), dma, dma((n_tp,)), dma((n_tp,)),
        ],
        compiler_params=pltpu.CompilerParams(
            collective_id=0, has_side_effects=True, vmem_limit_bytes=48 * 1024 * 1024
        ),
    )(
        latent, context, conditioning[None], context_conditioning[None],
        shift_weight, scale_weight, gate_weight, norm_gain[None],
        query_weight, key_weight, value_weight,
        jnp.tile(query_gain, 2)[None], jnp.tile(key_gain, 2)[None],
        cos_t.reshape(n_tp, rows, 128), sin_t.reshape(n_tp, rows, 128),
    )
    chunks = max(n_sp // 2, 2)
    o_rows = output_weight.shape[0]
    by_rows, wo_all = pl.pallas_call(
        functools.partial(attend_kernel, n_sp, n_tp, n_x, q_heads, k_heads, chunks),
        name="attend",
        out_shape=(
            jax.ShapeDtypeStruct((n_tp, rows, q_heads * HEAD), BF16),
            jax.ShapeDtypeStruct((n_tp, chunks, o_rows // chunks, model), BF16),
        ),
        in_specs=[vmem, vmem, vmem, pl.BlockSpec(memory_space=pltpu.SMEM), vmem],
        out_specs=(vmem, pl.BlockSpec(memory_space=pl.ANY)),
        scratch_shapes=[
            VMEM((n_sp // 2 + 1, length, 2 * k_width), BF16),
            VMEM((n_sp // 2, length, 2 * k_width), BF16),
            VMEM((n_sp, c_rows, 2 * k_width), BF16),
            VMEM((q_heads, length, 128), F32),
            VMEM((q_heads, length, 256), F32),
            VMEM((n_tp, rows, q_heads * HEAD), BF16),
            dma((2, n_sp)), dma((2, n_sp)), dma((2, n_sp)), dma((2, n_sp)),
            dma((n_tp, chunks)), dma((n_tp, chunks)), dma((n_tp, chunks)), dma((n_tp, chunks)),
            dma((n_tp,)), dma((n_tp,)), dma((3,)),
        ],
        compiler_params=pltpu.CompilerParams(
            collective_id=1, has_side_effects=True, vmem_limit_bytes=56 * 1024 * 1024
        ),
    )(
        qz.reshape(q_heads, length, 128), kv.reshape(length, 2 * k_width), ckv, context_lift,
        output_weight.reshape(chunks, o_rows // chunks, model),
    )
    projection = jnp.dot(
        jnp.transpose(by_rows, (1, 0, 2)).reshape(rows, n_tp * o_rows),
        wo_all.reshape(n_tp * o_rows, model),
        preferred_element_type=F32,
    )
    return (latent.astype(F32) + gate * projection).astype(BF16)


def solution(mesh):
    try:
        n_x = len({d.coords[0] for d in mesh.devices[:, 0]})
    except AttributeError:
        n_x = 1
    n_sp, n_tp = mesh.shape["sp"], mesh.shape["tp"]
    if n_x < 2 or n_sp % n_x or (n_sp // n_x) % 2:
        n_x = 1
    in_specs = (
        P(("sp", "tp"), None), P("sp", None), P("sp"), P("sp"),
        P("sp", "tp"), P("sp", "tp"), P("sp", "tp"), P(),
        P(None, "tp"), P(None, "tp"), P(None, "tp"), P(), P(), P("tp"), P("tp", None),
    )
    body = functools.partial(shards, n_sp, n_tp, n_x)
    return jax.shard_map(body, mesh=mesh, in_specs=in_specs, out_specs=P(("sp", "tp"), None), check_vma=False)
```

time: 282 us -> 141 us (0.50)
  Pallas kernels: 0 us -> 119 us
  blocking collectives: 84.3 us -> 0 us
  matrix products: 81.5 us -> 5.46 us
  other arithmetic: 44.6 us -> 0.42 us
  waiting for transfers between devices: 42.1 us -> 0 us
  between operations: 13.5 us -> 0.16 us
    pallas_call x0 -> x2, Pallas kernels: none -> 119 us  [the longest x1 90.7 us: shards(): pl.pallas_call(functools.partial(attend_kernel, n_sp, n_tp, n_x, q_heads,...]
    dot_general x15 -> x1, matrix products: 81.5 us -> 5.46 us  [shards(): jnp.dot(jnp.transpose(by_rows, (1, 0, 2)).reshape(rows, n_tp * o_rows), w...]
    all_gather x2 -> x0, blocking collectives: 41.4 us -> none  [the longest x1 28.6 us: shards(): lax.all_gather(jnp.concatenate([context_keys.astype(jnp.bfloat16).reshape...]
    all_gather x3 -> x0, waiting for transfers between devices: 41.4 us -> none  [the longest x1 23.7 us: shards(): piece = lax.all_gather(packed, 'sp', axis=0, tiled=True)]
    psum x1 -> x0, blocking collectives: 31 us -> none  [shards(): summed = lax.psum(partial_terms, 'sp')]
    reduce_sum x6 -> x0, other arithmetic: 30.5 us -> none  [the longest x3 29 us: absorb(): total = total * factor + jnp.sum(weights, axis=-1)]
    all_to_all x1 -> x0, blocking collectives: 11.9 us -> none  [shards(): lax.all_to_all(attended, 'tp', split_axis=0, concat_axis=1, tiled=True)]
    unnamed x20 -> x28, local copies, waits for them, and re-layouts: 0.04 us -> 11.8 us
  transfers between devices with their start and end apart: 3 -> 0, of which waited for: 2 -> 0; matrix products, arithmetic and copies ran while one was open for 41% -> 0% of each run, Pallas kernels for 0% -> 0%
where the time goes in v1:
time: 141 us
  Pallas kernels  119 us (84%)
  local copies, waits for them, and re-layouts  15.4 us (11%)
  matrix products  5.46 us (4%)
    pallas_call x1, Pallas kernels, shards(): pl.pallas_call(functools.partial(attend_kernel, n_sp, n_tp, n_x, q_heads,...  90.7 us
    pallas_call x1, Pallas kernels, shards(): pl.pallas_call(functools.partial(project_kernel, n_sp, n_tp, q_heads, k_h...  28.6 us
    unnamed x28, local copies, waits for them, and re-layouts  11.8 us
    dot_general x1, matrix products, shards(): jnp.dot(jnp.transpose(by_rows, (1, 0, 2)).reshape(rows, n_tp * o_rows), w...  5.46 us

profile of v1, /device:TPU:1, one launch (start us, length us, event | category | flops | bytes accessed | tf_op | source)
XLA Modules:
  0.0 140.7 jit_solution(3894970473013237638)
XLA Ops:
  0.0 0.0 copy-start.1
  0.0 0.7 tile.14
  0.7 0.1 broadcast_in_dim_tile.6.q_gain
  0.8 0.7 tile.30
  1.5 0.1 broadcast_in_dim_tile.7.k_gain
  1.6 0.1 broadcast_multiply_fusion.2
  1.7 0.2 fusion.2
  1.9 0.1 reshape.97
  2.0 0.1 broadcast_multiply_fusion
  2.2 0.1 tile.35
  2.3 0.1 copy.17.sin_t
  2.5 0.1 tile.31
  2.6 0.1 tile.33
  2.7 0.1 copy.16.cos_t
  2.8 0.0 copy-start
  2.8 1.0 copy-done
  3.9 0.0 copy-start.2
  3.9 1.2 copy-done.2
  5.1 0.0 copy-start.3
  5.1 1.2 copy-done.3
  6.3 0.0 copy-start.6
  6.3 0.9 copy-done.6
  7.3 0.0 copy-start.7
  7.3 0.9 copy-done.7
  8.2 0.0 copy-start.8
  8.2 0.9 copy-done.8
  9.2 0.0 copy-start.9
  9.2 0.9 copy-done.9
  10.1 0.0 copy-start.11
  10.1 0.7 copy-done.11
  10.8 0.0 copy-start.12
  10.8 0.7 copy-done.12
  11.5 0.0 copy-start.13
  11.5 0.7 copy-done.13
  12.2 28.6 %project.1 = (bf16[8,4,128,128]{3,2,1,0:T(8,128)(2,1)S(1)}, bf16[4,128,512]{2,1,0:T(8,128)(2,1)S(1)}, bf16[64,512]{1,0:T(8,128)(2,1)S(1)}, f32[1,2048]{1,0:T(1,128)S(1)}) custom-call(bf16[128,2048]{1,0:T(8,128)(2,1)S(1)} %copy-done, bf16[64,2048]{1,0:T(8,128)(2,1)S(1)} %copy-done.6, f32[1,256]{1,0:T(1,128)S(1)} %bitcast.24, f32[1,256]{1,0:T(1,128)S(1)} %bitcast.25, ...), custom_call_target="tpu_custom_call" | custom-call | tf_op jit(solution)/shard_map/project/pallas_call | solution.py:465
  40.8 0.0 copy-start.4
  40.8 1.0 copy-done.4
  41.8 0.0 copy-start.5
  41.8 0.8 copy-done.5
  42.6 0.0 copy-start.10
  42.6 0.6 copy-done.10
  43.2 90.7 %attend.1 = (bf16[4,128,512]{2,1,0:T(8,128)(2,1)}, bf16[4,4,128,2048]{3,2,1,0:T(8,128)(2,1)}) custom-call(bf16[8,512,128]{2,1,0:T(8,128)(2,1)} %bitcast.20, bf16[512,512]{1,0:T(8,128)(2,1)} %bitcast.21, bf16[64,512]{1,0:T(8,128)(2,1)} %copy-done.10, f32[8]{0:T(128)} %lift.1, bf16[4,128,2048]{2,1,0:T(8,128)(2,1)} %bitcast.28), custom_call_target="tpu_custom_call" | custom-call | tf_op jit(solution)/shard_map/attend/pallas_call | solution.py:498
  133.9 1.3 copy.18
  135.2 0.0 copy-done.1
  135.3 5.5 %fusion.1 = bf16[128,2048]{1,0:T(8,128)(2,1)} fusion(bf16[128,2048]{0,1:T(8,128)(2,1)S(1)} %bitcast.27, bf16[2048,2048]{1,0:T(8,128)(2,1)} %bitcast.26, bf16[128,2048]{1,0:T(8,128)(2,1)S(1)} %copy-done.1, f32[2048]{0:T(1024)S(1)} %bitcast.23), kind=kOutput, calls=%fused_computation.2 | convolution fusion | flops 1074790400 | bytes 9969664 | tf_op jit(solution)/shard_map/dot_general | solution.py:525
  (7 shorter events, 0.2 us)
Async XLA Ops:
  0.0 135.2 %copy-start.1 = (bf16[128,2048]{1,0:T(8,128)(2,1)S(1)}, bf16[128,2048]{1,0:T(8,128)(2,1)}, u32[]{:S(2)}) copy-start(bf16[128,2048]{1,0:T(8,128)(2,1)} %latent.1) | copy-start | bytes 1572868
  2.8 1.0 copy-start
  3.9 1.2 copy-start.2
  5.1 1.2 copy-start.3
  6.3 0.9 copy-start.6
  7.3 0.9 copy-start.7
  8.2 0.9 copy-start.8
  9.2 0.9 copy-start.9
  10.1 0.7 copy-start.11
  10.8 0.7 copy-start.12
  11.5 0.7 copy-start.13
  40.8 1.0 copy-start.4
  41.8 0.8 copy-start.5
  42.6 0.6 copy-start.10

commit v2 on v1

--- a/solution.py
+++ b/solution.py
@@ -33,12 +33,24 @@
 
 def project_kernel(
     n_sp, n_tp, q_heads, k_heads,
-    latent, context, cond, ctx_cond, shift_w, scale_w, gate_w, gain,
-    wq, wk, wv, q_gain, k_gain, cos_t, sin_t,
-    qz, kv, ckv, gate_out,
-    lat, part, total, recv1, recv2, mods,
-    s1, r1, s2, r2, sy, ry, sp_own, sp_fwd, rp,
+    latent_h, context_h, cond, ctx_cond, shift_h, scale_h, gate_h, gain,
+    wq_h, wk_h, wv_h, q_gain, k_gain, cos_t, sin_t,
+    qz, kv, call, gate_out,
+    latent, context, shift_w, scale_w, gate_w, wq, wk, wv,
+    lat, ckv, part, total, recv1, recv2, mods,
+    s1, r1, s2, r2, sy, ry, sp_own, sp_fwd, rp, sc, rc, loads,
 ):
+    fetch = [
+        pltpu.make_async_copy(src, dst, loads.at[i])
+        for i, (src, dst) in enumerate(
+            (
+                (latent_h, latent), (shift_h, shift_w), (scale_h, scale_w), (gate_h, gate_w),
+                (context_h, context), (wk_h, wk), (wv_h, wv), (wq_h, wq),
+            )
+        )
+    ]
+    for copy in fetch:
+        copy.start()
     me = lax.axis_index("sp")
     t = lax.axis_index("tp")
     n_y = n_tp // 2
@@ -57,6 +69,7 @@
     lax.fori_loop(1, n_sp, greet_sp, 0)
     lax.fori_loop(1, n_tp, greet_tp, 0)
     pl.semaphore_wait(barrier, n_sp + n_tp - 2)
+    fetch[0].wait()
 
     def y_copy(k):
         other = lax.rem(y + k, n_y)
@@ -76,6 +89,8 @@
     first = jnp.where(rows == 0, a, jnp.where(rows == 1, b, 0.0)).astype(BF16)
     second = jnp.where(rows == 2, a, jnp.where(rows == 3, b, 0.0)).astype(BF16)
     third = jnp.where(rows == 4, a, 0.0).astype(BF16)
+    for copy in fetch[1:4]:
+        copy.wait()
     mine = dot(first, shift_w[...]) + dot(second, scale_w[...]) + dot(third, gate_w[...])
     part[...] = mine
     recv1[me] = mine
@@ -148,10 +163,12 @@
     k_width = wk.shape[1]
     group = q_heads // k_heads
 
-    def process(tile, x):
+    def process(tiles, x):
         h = hidden_of(x, 0, 2)
-        cos_v, sin_v = cos_t[tile], sin_t[tile]
+        cos_v = jnp.concatenate([cos_t[tile] for tile in tiles], axis=0)
+        sin_v = jnp.concatenate([sin_t[tile] for tile in tiles], axis=0)
         q = turn(head_norm(dot(h, wq[...]), q_gain[...]), cos_v, sin_v)
+        per = q.shape[0] // len(tiles)
         low_half = lax.broadcasted_iota(jnp.int32, (q.shape[0], 128), 1) < HEAD
         for head in range(q_heads):
             piece = q[:, (head // 2) * 128 : (head // 2) * 128 + 128].astype(BF16).astype(F32) * HEAD ** (-0.5)
@@ -159,30 +176,55 @@
             if head % 2 != side:
                 piece = pltpu.roll(piece, HEAD, 1)
             keep = low_half if side == 0 else jnp.logical_not(low_half)
-            qz[head, tile] = jnp.where(keep, piece, 0.0).astype(BF16)
+            piece = jnp.where(keep, piece, 0.0)
+            for i, tile in enumerate(tiles):
+                qz[head, tile] = piece[i * per : (i + 1) * per].astype(BF16)
         k = turn(head_norm(dot(h, wk[...]), k_gain[...]), cos_v, sin_v)
-        kv[tile, :, :k_width] = k.astype(BF16)
-        kv[tile, :, k_width:] = dot(h, wv[...]).astype(BF16)
-
+        v = dot(h, wv[...])
+        for i, tile in enumerate(tiles):
+            kv[tile, :, :k_width] = k[i * per : (i + 1) * per].astype(BF16)
+            kv[tile, :, k_width:] = v[i * per : (i + 1) * per].astype(BF16)
+
+    for copy in fetch[4:]:
+        copy.wait()
     hc = hidden_of(context[...], 1, 3)
     ckv[:, :k_width] = head_norm(dot(hc, wk[...]), k_gain[...]).astype(BF16)
     ckv[:, k_width:] = dot(hc, wv[...]).astype(BF16)
 
-    process(t, latent[...])
+    def c_copy(j):
+        return remote(ckv, call.at[me], sc.at[j], rc.at[me], lax.rem(me + j, n_sp), t)
+
+    def c_start(j, _):
+        c_copy(j).start()
+        return 0
+
+    lax.fori_loop(1, n_sp, c_start, 0)
+    call[me] = ckv[...]
+
+    def pair_of(first, second):
+        return jnp.concatenate([first.astype(F32), second.astype(F32)], axis=0)
+
     pltpu.make_async_copy(lat.at[partner], lat.at[partner], rp.at[partner]).wait()
-    process(partner, lat[partner])
+    process((t, partner), pair_of(latent[...], lat[partner]))
 
     def others(k, _):
         other = lax.rem(y + n_y - k, n_y)
         near, far = other * 2 + c, other * 2 + 1 - c
         pltpu.make_async_copy(lat.at[near], lat.at[near], ry.at[near]).wait()
         remote(lat.at[near], lat.at[near], sp_fwd.at[k], rp.at[near], me, partner).start()
-        process(near, lat[near])
         pltpu.make_async_copy(lat.at[far], lat.at[far], rp.at[far]).wait()
-        process(far, lat[far])
+        process((near, far), pair_of(lat[near], lat[far]))
         return 0
 
     lax.fori_loop(1, n_y, others, 0)
+
+    def c_wait(j, _):
+        src = lax.rem(me + j, n_sp)
+        pltpu.make_async_copy(call.at[src], call.at[src], rc.at[src]).wait()
+        c_copy(j).wait_send()
+        return 0
+
+    lax.fori_loop(1, n_sp, c_wait, 0)
 
     def drain_y(k, _):
         y_copy(k).wait_send()
@@ -222,10 +264,10 @@
 
 def attend_kernel(
     n_sp, n_tp, n_x, q_heads, k_heads, chunks,
-    qz, kv, ckv, lift, wo,
+    qz, kv, call, lift, wo,
     by_rows, wo_all,
-    right, left, cbuf, m_ref, acc, att,
-    s_kv, r_kv, s_c, r_c, s_wy, r_wy, s_wp, r_wp, s_a, r_a, loc,
+    right, left, m_ref, acc, att,
+    s_kv, r_kv, s_wy, r_wy, s_wp, r_wp, s_a, r_a, loc,
 ):
     me = lax.axis_index("sp")
     t = lax.axis_index("tp")
@@ -257,30 +299,19 @@
     def hop(src, dst, direction, i):
         return remote(src, dst, s_kv.at[direction, i], r_kv.at[direction, i], nxt if direction == 0 else prv, t)
 
-    def chop(src, dst, direction, i):
-        return remote(src, dst, s_c.at[direction, i], r_c.at[direction, i], nxt if direction == 0 else prv, t)
-
-    def sends(i, source_r, source_l, c_r, c_l):
-        return (
-            hop(source_r, right.at[i], 0, i),
-            hop(source_l, left.at[i], 1, i),
-            chop(c_r, cbuf.at[i], 0, i),
-            chop(c_l, cbuf.at[n_sp - i], 1, i),
-        )
-
-    def last_sends(source_r, source_l, c_r):
+    def sends(i, source_r, source_l):
+        return (hop(source_r, right.at[i], 0, i), hop(source_l, left.at[i], 1, i))
+
+    def last_sends(source_r, source_l):
         return (
             hop(source_r.at[pl.ds(0, mid)], right.at[half, pl.ds(0, mid)], 0, half),
             hop(source_l.at[pl.ds(mid, mid)], right.at[half, pl.ds(mid, mid)], 1, half),
-            chop(c_r, cbuf.at[half], 0, half),
         )
 
-    opening = sends(1, kv, kv, ckv, ckv)
+    opening = sends(1, kv, kv)
     for copy in opening:
         copy.start()
-    own_c = pltpu.make_async_copy(ckv, cbuf.at[0], loc.at[0])
-    own_c.start()
-    own_w = pltpu.make_async_copy(wo, wo_all.at[t], loc.at[1])
+    own_w = pltpu.make_async_copy(wo, wo_all.at[t], loc.at[0])
     own_w.start()
 
     def w_y(k, ch):
@@ -314,54 +345,58 @@
     tiles = length // tile
 
     def attend(blocks, start, lifted):
-        def one(step, _):
-            head = step // tiles
-            row = pl.multiple_of(lax.rem(step, tiles) * tile, tile)
-            pair = head // (2 * group)
-            lane = pl.multiple_of(pair * 128, 128)
-            q = qz[head, pl.ds(row, tile), :]
+        def one(head, _):
+            lane = pl.multiple_of(head // (2 * group) * 128, 128)
             extra = lift[head]
-            scores = []
-            for pos, block in enumerate(blocks):
-                s = lax.dot_general(
-                    q, block[:, pl.ds(lane, 128)], (((1,), (1,)), ((), ())), preferred_element_type=F32
-                )
-                scores.append(s)
-            tops = [jnp.max(s, axis=-1, keepdims=True) for s in scores]
-            if lifted:
-                tops[-1] = tops[-1] + extra
-            top = functools.reduce(jnp.maximum, tops)
-            if not start:
-                old = m_ref[head, pl.ds(row, tile), :]
-                top = jnp.maximum(old[:, 0:1], top)
-            out = None
-            for pos, block in enumerate(blocks):
-                base = top - extra if lifted and pos == len(blocks) - 1 else top
-                p = jnp.exp(scores[pos] - base).astype(BF16)
-                v = block[:, pl.ds(pl.multiple_of(k_width + lane, 128), 128)]
-                term = dot(p, jnp.concatenate([v, jnp.ones_like(v)], axis=1))
-                out = term if out is None else out + term
-            if not start:
-                wide = jnp.broadcast_to(top, old.shape)
-                f = jnp.exp(old - wide)
-                out = acc[head, pl.ds(row, tile), :] * jnp.concatenate([f, f], axis=1) + out
-                m_ref[head, pl.ds(row, tile), :] = wide
-            else:
-                m_ref[head, pl.ds(row, tile), :] = jnp.broadcast_to(top, (tile, 128))
-            acc[head, pl.ds(row, tile), :] = out
+            spans = [pl.ds(i * tile, tile) for i in range(tiles)]
+            olds = [] if start else [m_ref[head, span, :] for span in spans]
+            keys = [block[:, pl.ds(lane, 128)] for block in blocks]
+            values = [block[:, pl.ds(pl.multiple_of(k_width + lane, 128), 128)] for block in blocks]
+            values = [jnp.concatenate([v, jnp.ones_like(v)], axis=1) for v in values]
+            scores = [
+                [
+                    lax.dot_general(
+                        qz[head, span, :], k, (((1,), (1,)), ((), ())), preferred_element_type=F32
+                    )
+                    for k in keys
+                ]
+                for span in spans
+            ]
+            tops, outs = [], []
+            for i in range(tiles):
+                peaks = [jnp.max(s, axis=-1, keepdims=True) for s in scores[i]]
+                if lifted:
+                    peaks[-1] = peaks[-1] + extra
+                top = functools.reduce(jnp.maximum, peaks)
+                if not start:
+                    top = jnp.maximum(olds[i][:, 0:1], top)
+                out = None
+                for pos, s in enumerate(scores[i]):
+                    base = top - extra if lifted and pos == len(blocks) - 1 else top
+                    term = dot(jnp.exp(s - base).astype(BF16), values[pos])
+                    out = term if out is None else out + term
+                wide = jnp.broadcast_to(top, (tile, 128))
+                if not start:
+                    f = jnp.exp(olds[i] - wide)
+                    out = acc[head, spans[i], :] * jnp.concatenate([f, f], axis=1) + out
+                tops.append(wide)
+                outs.append(out)
+            for i in range(tiles):
+                m_ref[head, spans[i], :] = tops[i]
+                acc[head, spans[i], :] = outs[i]
             return 0
 
-        lax.fori_loop(0, q_heads * tiles, one, 0)
+        lax.fori_loop(0, q_heads, one, 0)
 
     attend([kv], True, False)
 
     def wait_pair(i):
-        for copy in sends(i, kv, kv, ckv, ckv):
+        for copy in sends(i, kv, kv):
             copy.wait_recv()
 
     def step(i, _):
         wait_pair(i)
-        for copy in sends(i + 1, right.at[i], left.at[i], cbuf.at[i], cbuf.at[n_sp - i]):
+        for copy in sends(i + 1, right.at[i], left.at[i]):
             copy.start()
         attend([right.at[i], left.at[i]], False, False)
         forward_weight(i - 1)
@@ -369,7 +404,7 @@
 
     lax.fori_loop(1, half - 1, step, 0)
     wait_pair(half - 1)
-    closing = last_sends(right.at[half - 1], left.at[half - 1], cbuf.at[half - 1])
+    closing = last_sends(right.at[half - 1], left.at[half - 1])
     for copy in closing:
         copy.start()
     attend([right.at[half - 1], left.at[half - 1]], False, False)
@@ -377,9 +412,7 @@
         forward_weight(ch)
     for copy in closing:
         copy.wait_recv()
-    own_c.wait()
-    cflat = cbuf.reshape(n_sp * ckv.shape[0], ckv.shape[1])
-    attend([right.at[half], cflat], False, True)
+    attend([right.at[half], call], False, True)
 
     low_half = lax.broadcasted_iota(jnp.int32, (length, 128), 1) < HEAD
     per = length // n_tp
@@ -404,7 +437,7 @@
 
     for j in range(1, n_tp):
         a_copy(j).start()
-    own_a = pltpu.make_async_copy(att.at[t], by_rows.at[t], loc.at[2])
+    own_a = pltpu.make_async_copy(att.at[t], by_rows.at[t], loc.at[1])
     own_a.start()
     own_a.wait()
     for j in range(1, n_tp):
@@ -423,7 +456,7 @@
         a_copy(j).wait_send()
 
     def drain(i, _):
-        for copy in sends(i, kv, kv, ckv, ckv):
+        for copy in sends(i, kv, kv):
             copy.wait_send()
         return 0
 
@@ -462,19 +495,24 @@
     cos_t, sin_t = rotary_tables(lax.axis_index("sp") * length, length)
     vmem = pl.BlockSpec(memory_space=VMEM)
     dma = pltpu.SemaphoreType.DMA
-    qz, kv, ckv, gate = pl.pallas_call(
+    hbm = pl.BlockSpec(memory_space=pltpu.HBM)
+    qz, kv, call, gate = pl.pallas_call(
         functools.partial(project_kernel, n_sp, n_tp, q_heads, k_heads),
         name="project",
         out_shape=(
             jax.ShapeDtypeStruct((q_heads, n_tp, rows, 128), BF16),
             jax.ShapeDtypeStruct((n_tp, rows, 2 * k_width), BF16),
-            jax.ShapeDtypeStruct((c_rows, 2 * k_width), BF16),
+            jax.ShapeDtypeStruct((n_sp, c_rows, 2 * k_width), BF16),
             jax.ShapeDtypeStruct((1, model), F32),
         ),
-        in_specs=[vmem] * 15,
+        in_specs=[hbm, hbm, vmem, vmem, hbm, hbm, hbm, vmem, hbm, hbm, hbm, vmem, vmem, vmem, vmem],
         out_specs=(vmem,) * 4,
         scratch_shapes=[
+            VMEM(latent.shape, BF16), VMEM(context.shape, BF16),
+            VMEM(shift_weight.shape, BF16), VMEM(scale_weight.shape, BF16), VMEM(gate_weight.shape, BF16),
+            VMEM(query_weight.shape, BF16), VMEM(key_weight.shape, BF16), VMEM(value_weight.shape, BF16),
             VMEM((n_tp, rows, model), BF16),
+            VMEM((c_rows, 2 * k_width), BF16),
             VMEM((8, part_width), F32),
             VMEM((8, part_width), F32),
             VMEM((n_sp, 8, part_width), F32),
@@ -482,6 +520,7 @@
             VMEM((8, model), F32),
             dma((n_sp,)), dma((n_sp,)), dma((n_tp,)), dma((n_tp,)),
             dma((n_tp,)), dma((n_tp,)), dma, dma((n_tp,)), dma((n_tp,)),
+            dma((n_sp,)), dma((n_sp,)), dma((8,)),
         ],
         compiler_params=pltpu.CompilerParams(
             collective_id=0, has_side_effects=True, vmem_limit_bytes=48 * 1024 * 1024
@@ -507,19 +546,19 @@
         scratch_shapes=[
             VMEM((n_sp // 2 + 1, length, 2 * k_width), BF16),
             VMEM((n_sp // 2, length, 2 * k_width), BF16),
-            VMEM((n_sp, c_rows, 2 * k_width), BF16),
             VMEM((q_heads, length, 128), F32),
             VMEM((q_heads, length, 256), F32),
             VMEM((n_tp, rows, q_heads * HEAD), BF16),
-            dma((2, n_sp)), dma((2, n_sp)), dma((2, n_sp)), dma((2, n_sp)),
+            dma((2, n_sp)), dma((2, n_sp)),
             dma((n_tp, chunks)), dma((n_tp, chunks)), dma((n_tp, chunks)), dma((n_tp, chunks)),
-            dma((n_tp,)), dma((n_tp,)), dma((3,)),
+            dma((n_tp,)), dma((n_tp,)), dma((2,)),
         ],
         compiler_params=pltpu.CompilerParams(
             collective_id=1, has_side_effects=True, vmem_limit_bytes=56 * 1024 * 1024
         ),
     )(
-        qz.reshape(q_heads, length, 128), kv.reshape(length, 2 * k_width), ckv, context_lift,
+        qz.reshape(q_heads, length, 128), kv.reshape(length, 2 * k_width),
+        call.reshape(n_sp * c_rows, 2 * k_width), context_lift,
         output_weight.reshape(chunks, o_rows // chunks, model),
     )
     projection = jnp.dot(

time: 141 us -> 123 us (0.87)
  Pallas kernels: 119 us -> 102 us
    pallas_call x1, Pallas kernels: 90.7 us -> 72.2 us  [shards(): pl.pallas_call(functools.partial(attend_kernel, n_sp, n_tp, n_x, q_heads,...]
    unnamed x28 -> x26, local copies, waits for them, and re-layouts: 11.8 us -> 10.8 us
where the time goes in v2:
time: 123 us; the launch traced here: 122 us
  Pallas kernels  102 us (83%)
  local copies, waits for them, and re-layouts  14.4 us (12%)
  matrix products  5.46 us (4%)
    pallas_call x1, Pallas kernels, shards(): pl.pallas_call(functools.partial(attend_kernel, n_sp, n_tp, n_x, q_heads,...  72.2 us
    pallas_call x1, Pallas kernels, shards(): pl.pallas_call(functools.partial(project_kernel, n_sp, n_tp, q_heads, k_h...  29.8 us
    unnamed x26, local copies, waits for them, and re-layouts  10.8 us
    dot_general x1, matrix products, shards(): jnp.dot(jnp.transpose(by_rows, (1, 0, 2)).reshape(rows, n_tp * o_rows), w...  5.46 us

profile of v2, /device:TPU:1, one launch (start us, length us, event | category | flops | bytes accessed | tf_op | source)
XLA Modules:
  0.0 122.4 jit_solution(7354165130385573885)
XLA Ops:
  0.0 0.0 copy-start.1
  0.0 0.7 tile.14
  0.7 0.1 broadcast_in_dim_tile.6.q_gain
  0.8 0.7 tile.30
  1.5 0.1 broadcast_in_dim_tile.7.k_gain
  1.6 0.1 broadcast_multiply_fusion.2
  1.7 0.2 fusion.2
  1.9 0.1 reshape.100
  2.0 0.1 broadcast_multiply_fusion
  2.2 0.1 tile.35
  2.3 0.1 copy.17.sin_t
  2.5 0.1 tile.31
  2.6 0.1 tile.33
  2.7 0.1 copy.16.cos_t
  2.8 0.0 copy-start
  2.8 1.0 copy-done
  3.9 0.0 copy-start.2
  3.9 1.2 copy-done.2
  5.1 0.0 copy-start.6
  5.1 0.9 copy-done.6
  6.0 0.0 copy-start.7
  6.0 0.9 copy-done.7
  7.0 0.0 copy-start.8
  7.0 0.9 copy-done.8
  7.9 0.0 copy-start.9
  7.9 0.9 copy-done.9
  8.9 0.0 copy-start.10
  8.9 0.7 copy-done.10
  9.6 0.0 copy-start.11
  9.6 0.7 copy-done.11
  10.3 0.0 copy-start.12
  10.3 0.7 copy-done.12
  10.9 29.8 %project.1 = (bf16[8,4,128,128]{3,2,1,0:T(8,128)(2,1)S(1)}, bf16[4,128,512]{2,1,0:T(8,128)(2,1)S(1)}, bf16[8,64,512]{2,1,0:T(8,128)(2,1)S(1)}, f32[1,2048]{1,0:T(1,128)S(1)}) custom-call(bf16[128,2048]{1,0:T(8,128)(2,1)S(1)} %copy-done, bf16[64,2048]{1,0:T(8,128)(2,1)S(1)} %copy-done.6, f32[1,256]{1,0:T(1,128)S(1)} %bitcast.26, f32[1,256]{1,0:T(1,128)S(1)} %bitcast.27, ...), custom_call_target="tpu_custom_call" | custom-call | tf_op jit(solution)/shard_map/project/pallas_call | solution.py:499
  40.7 0.0 copy-start.3
  40.7 1.0 copy-done.3
  41.8 0.0 copy-start.4
  41.8 0.8 copy-done.4
  42.6 0.0 copy-start.5
  42.6 0.8 copy-done.5
  43.4 72.2 %attend.1 = (bf16[4,128,512]{2,1,0:T(8,128)(2,1)}, bf16[4,4,128,2048]{3,2,1,0:T(8,128)(2,1)}) custom-call(bf16[8,512,128]{2,1,0:T(8,128)(2,1)} %bitcast.21, bf16[512,512]{1,0:T(8,128)(2,1)} %bitcast.22, bf16[512,512]{1,0:T(8,128)(2,1)} %bitcast.23, f32[8]{0:T(128)} %lift.1, bf16[4,128,2048]{2,1,0:T(8,128)(2,1)} %bitcast.30), custom_call_target="tpu_custom_call" | custom-call | tf_op jit(solution)/shard_map/attend/pallas_call | solution.py:537
  115.6 1.3 %copy.18 = bf16[128,4,512]{0,2,1:T(8,128)(2,1)S(1)} copy(bf16[128,4,512]{2,0,1:T(8,128)(2,1)} %bitcast.31) | data formatting | bytes 1048576 | tf_op jit(solution)/shard_map/transpose | solution.py:565
  116.9 0.0 copy-done.1
  117.0 5.5 %fusion.1 = bf16[128,2048]{1,0:T(8,128)(2,1)} fusion(bf16[128,2048]{0,1:T(8,128)(2,1)S(1)} %bitcast.29, bf16[2048,2048]{1,0:T(8,128)(2,1)} %bitcast.28, bf16[128,2048]{1,0:T(8,128)(2,1)S(1)} %copy-done.1, f32[2048]{0:T(1024)S(1)} %bitcast.25), kind=kOutput, calls=%fused_computation.2 | convolution fusion | flops 1074790400 | bytes 9969664 | tf_op jit(solution)/shard_map/dot_general | solution.py:564
  (7 shorter events, 0.2 us)
Async XLA Ops:
  0.0 116.9 %copy-start.1 = (bf16[128,2048]{1,0:T(8,128)(2,1)S(1)}, bf16[128,2048]{1,0:T(8,128)(2,1)}, u32[]{:S(2)}) copy-start(bf16[128,2048]{1,0:T(8,128)(2,1)} %latent_h.1) | copy-start | bytes 1572868
  2.8 1.0 copy-start
  3.9 1.2 %copy-start.2 = (bf16[2048,256]{1,0:T(8,128)(2,1)S(1)}, bf16[2048,256]{1,0:T(8,128)(2,1)}, u32[]{:S(2)}) copy-start(bf16[2048,256]{1,0:T(8,128)(2,1)} %wk_h.1) | copy-start | bytes 3145732
  5.1 0.9 copy-start.6
  6.0 0.9 copy-start.7
  7.0 0.9 copy-start.8
  7.9 0.9 copy-start.9
  8.9 0.7 copy-start.10
  9.6 0.7 copy-start.11
  10.3 0.7 copy-start.12
  40.7 1.1 copy-start.3
  41.8 0.8 copy-start.4
  42.6 0.8 copy-start.5

commit v3 on v2

--- a/solution.py
+++ b/solution.py
@@ -523,7 +523,7 @@
             dma((n_sp,)), dma((n_sp,)), dma((8,)),
         ],
         compiler_params=pltpu.CompilerParams(
-            collective_id=0, has_side_effects=True, vmem_limit_bytes=48 * 1024 * 1024
+            collective_id=0, has_side_effects=True, vmem_limit_bytes=67043328
         ),
     )(
         latent, context, conditioning[None], context_conditioning[None],

time: 123 us -> 116 us (0.943)
  local copies, waits for them, and re-layouts: 14.4 us -> 5.98 us
  Pallas kernels: 102 us -> 104 us
    unnamed x26 -> x0, local copies, waits for them, and re-layouts: 10.8 us -> none
    pallas_call x1, Pallas kernels: 29.8 us -> 32 us  [shards(): pl.pallas_call(functools.partial(project_kernel, n_sp, n_tp, q_heads, k_h...]
    another operation x7, local copies, waits for them, and re-layouts: 0.57 us -> 1.99 us  [rotary_tables(): return (jnp.tile(cos_t, (1, 2)), jnp.tile(sin_t, (1, 2)))]
where the time goes in v3:
time: 116 us
  Pallas kernels  104 us (90%)
  local copies, waits for them, and re-layouts  5.98 us (5%)
  matrix products  5.65 us (5%)
    pallas_call x1, Pallas kernels, shards(): pl.pallas_call(functools.partial(attend_kernel, n_sp, n_tp, n_x, q_heads,...  71.6 us
    pallas_call x1, Pallas kernels, shards(): pl.pallas_call(functools.partial(project_kernel, n_sp, n_tp, q_heads, k_h...  32 us
    dot_general x1, matrix products, shards(): jnp.dot(jnp.transpose(by_rows, (1, 0, 2)).reshape(rows, n_tp * o_rows), w...  5.65 us

profile of v3, /device:TPU:1, one launch (start us, length us, event | category | flops | bytes accessed | tf_op | source)
XLA Modules:
  0.0 115.8 jit_solution(629375800311027166)
XLA Ops:
  0.0 0.7 tile.14
  0.7 0.6 broadcast_in_dim_tile.6.q_gain
  1.3 0.7 tile.30
  1.9 0.6 broadcast_in_dim_tile.7.k_gain
  2.5 0.1 broadcast_multiply_fusion.2
  2.6 0.2 fusion.2
  2.9 0.1 reshape.100
  3.0 0.1 broadcast_multiply_fusion
  3.1 0.1 tile.35
  3.2 0.8 copy.17.sin_t
  4.1 0.1 tile.31
  4.2 0.1 tile.33
  4.3 0.8 copy.16.cos_t
  5.2 32.0 %project.1 = (bf16[8,4,128,128]{3,2,1,0:T(8,128)(2,1)}, bf16[4,128,512]{2,1,0:T(8,128)(2,1)}, bf16[8,64,512]{2,1,0:T(8,128)(2,1)}, f32[1,2048]{1,0:T(1,128)}) custom-call(bf16[128,2048]{1,0:T(8,128)(2,1)} %latent_h.1, bf16[64,2048]{1,0:T(8,128)(2,1)} %context_h.1, f32[1,256]{1,0:T(1,128)} %bitcast.30, f32[1,256]{1,0:T(1,128)} %bitcast.31, ...), custom_call_target="tpu_custom_call" | custom-call | tf_op jit(solution)/shard_map/project/pallas_call | solution.py:499
  37.1 71.6 %attend.1 = (bf16[4,128,512]{2,1,0:T(8,128)(2,1)}, bf16[4,4,128,2048]{3,2,1,0:T(8,128)(2,1)}) custom-call(bf16[8,512,128]{2,1,0:T(8,128)(2,1)} %bitcast.24, bf16[512,512]{1,0:T(8,128)(2,1)} %bitcast.25, bf16[512,512]{1,0:T(8,128)(2,1)} %bitcast.26, f32[8]{0:T(128)} %lift.1, bf16[4,128,2048]{2,1,0:T(8,128)(2,1)} %bitcast.23), custom_call_target="tpu_custom_call" | custom-call | tf_op jit(solution)/shard_map/attend/pallas_call | solution.py:537
  108.8 1.3 %copy.18 = bf16[128,4,512]{0,2,1:T(8,128)(2,1)S(1)} copy(bf16[128,4,512]{2,0,1:T(8,128)(2,1)} %bitcast.27) | data formatting | bytes 1048576 | tf_op jit(solution)/shard_map/transpose | solution.py:565
  110.1 5.7 %fusion.1 = bf16[128,2048]{1,0:T(8,128)(2,1)} fusion(bf16[128,2048]{0,1:T(8,128)(2,1)S(1)} %bitcast.22, bf16[2048,2048]{1,0:T(8,128)(2,1)} %bitcast.21, bf16[128,2048]{1,0:T(8,128)(2,1)} %latent_h.1, f32[2048]{0:T(1024)} %bitcast.29), kind=kOutput, calls=%fused_computation.2 | convolution fusion | flops 1074790400 | bytes 9969664 | tf_op jit(solution)/shard_map/dot_general | solution.py:564
  (7 shorter events, 0.2 us)
